TPU v7x, 32 devices: a whole 2x2x4 slice. The times are simulated.
32 devices in a mesh: ep: 8 (over z, core), tp: 4 (over y, x).
Axes of the slice: x: 2, y: 2, z: 4, core: 2. Of those that a mesh axis runs over, the one named last changes fastest.
Arguments:
- tokens: bfloat16 [256, 2048], P('ep'), may hold values from -6 to 6
- recurrent_head_state: float32 [256, 16, 4096], P('ep', 'tp'), may hold values from -4 to 4
- first_norm_gain: float32 [2048], replicated, may hold values from 0.1 to 1.9
- receptance_matrix: bfloat16 [2048, 1024], P(None, 'tp'), may hold values from -0.125 to 0.125
- key_matrix: bfloat16 [2048, 1024], P(None, 'tp'), may hold values from -0.125 to 0.125
- value_matrix: bfloat16 [2048, 1024], P(None, 'tp'), may hold values from -0.125 to 0.125
- decay_matrix: bfloat16 [2048, 1024], P(None, 'tp'), may hold values from -0.125 to 0.125
- decay_offset: float32 [1024], P('tp'), may hold values from -3 to 0.5
- correction_offset: float32 [1024], P('tp'), may hold values from -2 to 2
- correction_key_factor: float32 [1024], P('tp'), may hold values from -1 to 1
- own_term_weight: float32 [1024], P('tp'), may hold values from -0.9 to 0.9
- head_norm_gain: float32 [1024], P('tp'), may hold values from 0.1 to 1.9
- output_matrix: bfloat16 [1024, 2048], P('tp'), may hold values from -0.1875 to 0.1875
- second_norm_gain: float32 [2048], replicated, may hold values from 0.1 to 1.9
- routing: int32 [256, 2], replicated, may hold values from 0 to 7, all different within a row; in each aligned block of 32 rows (0 to 31, 32 to 63, ...) at most 16 rows name the same one
- routing_weight: float32 [256, 2], P('ep'), may hold values from 0.1 to 1
- expert_gate_weight: bfloat16 [8, 2048, 4096], P('ep', None, 'tp'), may hold values from -0.125 to 0.125
- expert_up_weight: bfloat16 [8, 2048, 4096], P('ep', None, 'tp'), may hold values from -0.125 to 0.125
- expert_down_weight: bfloat16 [8, 4096, 2048], P('ep', 'tp'), may hold values from -0.125 to 0.125
- dense_gate_weight: bfloat16 [2048, 2816], P(None, 'ep'), may hold values from -0.125 to 0.125
- dense_up_weight: bfloat16 [2048, 2816], P(None, 'ep'), may hold values from -0.125 to 0.125
- dense_down_weight: bfloat16 [2816, 2048], P('ep'), may hold values from -0.109375 to 0.109375
- dense_gate_offset: float32 [2048], replicated, may hold values from -3 to 3
Outputs:
- layer_out: bfloat16 [256, 2048], P(('ep', 'tp'))
- next_state: float32 [256, 16, 4096], P('ep', 'tp')
Inputs may be any that keep to these rules, and one draw needn't show every extreme that they name: `routing`: each row names 2 different experts. In each aligned block of 32 rows no expert is named more than 16 times, a bound that some block reaches.
All inputs are finite; a program needn't handle non-finite values.
Results may differ from a plain program's by a relative error of at most 0.017.
Values may be sent and summed in bfloat16 or wider, within the bound.
A program may use at most 64 MiB of HBM per device.

v0:
```python
import jax
import jax.numpy as jnp
from jax import lax
from jax.sharding import PartitionSpec as P

HEAD_WIDTH = 64


PRECISE = lax.Precision.HIGHEST


def rms_scale(rows, gain):
    floats = rows.astype(jnp.float32)
    return floats * lax.rsqrt(jnp.mean(floats * floats, axis=-1, keepdims=True) + 1e-06) * gain


def route_table(block_routes, experts, capacity):
    flat_routes = block_routes.reshape(-1)
    chosen = (flat_routes[:, None] == jnp.arange(experts, dtype=jnp.int32)[None, :]).astype(
        jnp.int32
    )
    before = jnp.cumsum(chosen, axis=0, dtype=jnp.int32) - chosen
    slot_index = jnp.sum(before * chosen, axis=1)
    slot_match = (slot_index[:, None] == jnp.arange(capacity, dtype=jnp.int32)[None, :]).astype(
        jnp.float32
    )
    dispatch_table = chosen.astype(jnp.float32)[:, :, None] * slot_match[:, None, :]
    return dispatch_table.reshape(block_routes.shape[0], block_routes.shape[1], experts, capacity)


def state_update(
    receptance_rows,
    key_matrix_rows,
    value_matrix_rows,
    decay_logits,
    recurrent_head_state,
    decay_offset,
    correction_offset,
    correction_key_factor,
    own_term_weight,
    head_norm_gain,
    head_width,
):
    seq_count = key_matrix_rows.shape[0]
    decay_factor = jnp.exp(-jnp.exp(decay_offset + decay_logits))
    in_rate = jax.nn.sigmoid(correction_offset + correction_key_factor * key_matrix_rows)
    key_in = key_matrix_rows * in_rate

    def split_heads(block):
        return block.reshape(seq_count, -1, head_width)

    keys_head = split_heads(key_matrix_rows)
    unit_keys = (
        keys_head
        * lax.rsqrt(jnp.mean(keys_head * keys_head, axis=-1, keepdims=True) + 1e-06)
        * head_width ** (-0.5)
    )
    rate_head = split_heads(in_rate)
    head_keys = split_heads(key_in)
    decay_head = split_heads(decay_factor)
    head_values = split_heads(value_matrix_rows)
    head_receptance = split_heads(receptance_rows)
    matrix = recurrent_head_state.reshape(seq_count, -1, head_width, head_width)
    removed = jnp.einsum("bhvk,bhk->bhv", matrix, unit_keys, precision=PRECISE)
    updated = (
        matrix * decay_head[:, :, None, :]
        - removed[..., None] * (unit_keys * rate_head)[:, :, None, :]
        + head_values[..., None] * head_keys[:, :, None, :]
    )
    readout = jnp.einsum("bhvk,bhk->bhv", updated, head_receptance, precision=PRECISE)
    center = jnp.mean(readout, axis=-1, keepdims=True)
    spread = jnp.mean(jnp.square(readout - center), axis=-1, keepdims=True)
    normalized_rows = (
        (readout - center) * lax.rsqrt(spread + 0.00064) * head_norm_gain.reshape(-1, head_width)
    )
    own_term_total = jnp.sum(
        head_receptance * head_keys * own_term_weight.reshape(-1, head_width),
        axis=-1,
        keepdims=True,
    )
    normalized_rows = normalized_rows + own_term_total * head_values
    return (
        normalized_rows.reshape(seq_count, -1).astype(jnp.bfloat16),
        updated.reshape(seq_count, -1, head_width * head_width),
    )


def local(
    tokens,
    recurrent_head_state,
    first_norm_gain,
    receptance_matrix,
    key_matrix,
    value_matrix,
    decay_matrix,
    decay_offset,
    correction_offset,
    correction_key_factor,
    own_term_weight,
    head_norm_gain,
    output_matrix,
    second_norm_gain,
    routing,
    routing_weight,
    expert_gate_weight,
    expert_up_weight,
    expert_down_weight,
    dense_gate_weight,
    dense_up_weight,
    dense_down_weight,
    dense_gate_offset,
):
    seq_count = tokens.shape[0]
    width = tokens.shape[1]
    group_index = lax.axis_index("ep")
    lane_index = lax.axis_index("tp")
    group_count = lax.axis_size("ep")
    lane_count = lax.axis_size("tp")
    normalized_rows = rms_scale(tokens, first_norm_gain).astype(jnp.bfloat16)
    receptance_rows = jnp.dot(
        normalized_rows, receptance_matrix, preferred_element_type=jnp.float32
    )
    key_matrix_rows = jnp.dot(normalized_rows, key_matrix, preferred_element_type=jnp.float32)
    value_matrix_rows = jnp.dot(normalized_rows, value_matrix, preferred_element_type=jnp.float32)
    decay_logits = jnp.dot(normalized_rows, decay_matrix, preferred_element_type=jnp.float32)
    head_outputs, next_state = state_update(
        receptance_rows,
        key_matrix_rows,
        value_matrix_rows,
        decay_logits,
        recurrent_head_state,
        decay_offset,
        correction_offset,
        correction_key_factor,
        own_term_weight,
        head_norm_gain,
        HEAD_WIDTH,
    )
    partial_out = jnp.dot(head_outputs, output_matrix, preferred_element_type=jnp.float32)
    hidden_sum = tokens.astype(jnp.float32) + lax.psum(
        partial_out.astype(jnp.bfloat16), "tp"
    ).astype(jnp.float32)
    ffn_in = rms_scale(hidden_sum, second_norm_gain).astype(jnp.bfloat16)
    local_experts = expert_gate_weight.shape[0]
    top_count = routing.shape[1]
    expert_count = local_experts * group_count
    capacity = 2 * seq_count * top_count // expert_count
    per_lane = seq_count // lane_count
    own_routes = lax.dynamic_slice_in_dim(routing, group_index * seq_count, seq_count, 0)
    own_table = route_table(own_routes, expert_count, capacity)
    send_rows = jnp.einsum(
        "bkec,bd->ecd", own_table.astype(jnp.bfloat16), ffn_in, preferred_element_type=jnp.float32
    ).astype(jnp.bfloat16)
    lane_rows = lax.dynamic_slice_in_dim(ffn_in, lane_index * per_lane, per_lane, 0)
    dense_send = jnp.broadcast_to(lane_rows[None], (group_count, per_lane, width))
    expert_in, dense_in = (
        lax.all_to_all(send_rows, "ep", split_axis=0, concat_axis=0, tiled=True),
        lax.all_to_all(dense_send, "ep", split_axis=0, concat_axis=0, tiled=True),
    )
    rows_in = expert_in.reshape(group_count, local_experts, capacity, width).transpose(1, 0, 2, 3)
    rows_in = rows_in.reshape(local_experts, group_count * capacity, width)
    gate_pre = jnp.einsum(
        "lrd,ldf->lrf", rows_in, expert_gate_weight, preferred_element_type=jnp.float32
    )
    up_pre = jnp.einsum(
        "lrd,ldf->lrf", rows_in, expert_up_weight, preferred_element_type=jnp.float32
    )
    expert_hidden = (jax.nn.silu(gate_pre) * up_pre).astype(jnp.bfloat16)
    expert_part = jnp.einsum(
        "lrf,lfd->lrd", expert_hidden, expert_down_weight, preferred_element_type=jnp.float32
    )
    expert_out = lax.psum_scatter(
        expert_part.astype(jnp.bfloat16), "tp", scatter_dimension=2, tiled=True
    )
    back_send = expert_out.reshape(local_experts, group_count, capacity, -1).transpose(1, 0, 2, 3)
    back_send = back_send.reshape(group_count * local_experts, capacity, -1)
    dense_rows = dense_in.reshape(group_count * per_lane, width)
    dense_hidden = (
        jax.nn.silu(jnp.dot(dense_rows, dense_gate_weight, preferred_element_type=jnp.float32))
        * jnp.dot(dense_rows, dense_up_weight, preferred_element_type=jnp.float32)
    ).astype(jnp.bfloat16)
    dense_part = jnp.dot(
        dense_hidden, dense_down_weight, preferred_element_type=jnp.float32
    ).astype(jnp.bfloat16)
    dense_part = dense_part.reshape(group_count, per_lane, width)
    back_experts, back_dense = (
        lax.all_to_all(back_send, "ep", split_axis=0, concat_axis=0, tiled=True),
        lax.all_to_all(dense_part, "ep", split_axis=0, concat_axis=0, tiled=True),
    )
    dense_sum = jnp.sum(back_dense.astype(jnp.float32), axis=0)
    weighted = jnp.einsum("bkec,bk->ecb", own_table, routing_weight, precision=PRECISE)
    moe_slice = jnp.einsum(
        "ecb,ecd->bd", weighted, back_experts.astype(jnp.float32), precision=PRECISE
    )
    moe_rows = lax.all_to_all(moe_slice, "tp", split_axis=0, concat_axis=1, tiled=True)
    residual_rows = lax.dynamic_slice_in_dim(hidden_sum, lane_index * per_lane, per_lane, 0)
    layer_out = (residual_rows + moe_rows + jax.nn.sigmoid(dense_gate_offset) * dense_sum).astype(
        jnp.bfloat16
    )
    return (layer_out, next_state)


def solution(mesh):
    return jax.shard_map(
        local,
        mesh=mesh,
        in_specs=(
            P("ep", None),
            P("ep", "tp", None),
            P(),
            P(None, "tp"),
            P(None, "tp"),
            P(None, "tp"),
            P(None, "tp"),
            P("tp"),
            P("tp"),
            P("tp"),
            P("tp"),
            P("tp"),
            P("tp", None),
            P(),
            P(),
            P("ep", None),
            P("ep", None, "tp"),
            P("ep", None, "tp"),
            P("ep", "tp", None),
            P(None, "ep"),
            P(None, "ep"),
            P("ep", None),
            P(),
        ),
        out_specs=(P(("ep", "tp"), None), P("ep", "tp", None)),
        check_vma=False,
    )
```

profile of v0, /device:TPU:0, one launch (start us, length us, event | category | flops | bytes accessed | tf_op | source)
XLA Modules:
  0.0 217.0 jit_solution(15776234293525649654)
XLA Ops:
  8.5 2.3 %fusion.62 = f32[32,256]{1,0:T(8,128)} fusion(bf16[2048,256]{1,0:T(8,128)(2,1)} %param.26, bf16[32,2048]{1,0:T(8,128)(2,1)} %param.23, f32[2048]{0:T(1024)} %param.25, f32[32]{0:T(128)S(1)} %add_rsqrt_fusion.3), kind=kOutput, calls=%fused_computation.88 | convolution fusion | flops 33816576 | bytes 1220736 | tf_op jit(solution)/shard_map/dot_general | solution.py:120
  16.4 2.3 %fusion.64 = f32[32,256]{1,0:T(8,128)} fusion(bf16[2048,256]{1,0:T(8,128)(2,1)} %param.28, bf16[32,2048]{1,0:T(8,128)(2,1)} %param.23, f32[2048]{0:T(1024)} %param.25, f32[32]{0:T(128)S(1)} %add_rsqrt_fusion.3), kind=kOutput, calls=%fused_computation.89 | convolution fusion | flops 33816576 | bytes 1220736 | tf_op jit(solution)/shard_map/dot_general | solution.py:124
  20.1 2.3 %fusion.31 = f32[32,256]{1,0:T(8,128)} fusion(bf16[2048,256]{1,0:T(8,128)(2,1)} %param.29, f32[256]{0:T(256)} %param.30, bf16[32,2048]{1,0:T(8,128)(2,1)} %param.23, f32[2048]{0:T(1024)} %param.25, f32[32]{0:T(128)S(1)} %add_rsqrt_fusion.3), kind=kOutput, calls=%fused_computation.32 | convolution fusion | flops 33832960 | bytes 1221760 | tf_op jit(solution)/shard_map/dot_general | solution.py:125
  23.8 2.2 %fusion.61 = (f32[32,256]{1,0:T(8,128)}, f32[32,256]{1,0:T(8,128)}, f32[32,256]{1,0:T(8,128)}) fusion(f32[256]{0:T(256)S(1)} %copy-done.13, f32[256]{0:T(256)} %param.31, bf16[2048,256]{1,0:T(8,128)(2,1)} %param.27, bf16[32,2048]{1,0:T(8,128)(2,1)} %param.23, f32[2048]{0:T(1024)S(1)} %copy-done.10, f32[32]{0:T(128)S(1)} %add_rsqrt_fusion.3), kind=kOutput, calls=%fused_computation.87 | convolution fusion | flops 33865728 | bytes 1288320 | tf_op jit(solution)/shard_map/dot_general | solution.py:123
  31.4 3.3 %reshape.173 = f32[32,4,64,64]{3,2,1,0:T(8,128)} reshape(f32[32,4,4096]{2,1,0:T(4,128)S(1)} %copy-done.2) | data formatting | bytes 4194304 | tf_op jit(solution)/shard_map/reshape | solution.py:63
  35.9 8.6 %fusion.70 = f32[32,4,1,64]{3,2,1,0:T(1,128)S(1)} fusion(f32[32,4,64,1]{2,3,1,0:T(1,128)S(1)} %bitcast.86, f32[32,4,64,64]{3,2,1,0:T(8,128)} %reshape.173), kind=kOutput, calls=%fused_computation.92 | convolution fusion | flops 6291456 | bytes 2162688 | tf_op jit(solution)/shard_map/bhvk,bhk->bhv/dot_general | solution.py:64
  44.5 9.0 %fusion.7 = f32[32,4,1,64]{3,2,1,0:T(1,128)} fusion(f32[32,4,64,1]{2,3,1,0:T(1,128)S(1)} %bitcast.92, f32[32,4,64,64]{3,2,1,0:T(8,128)S(1)} %copy-done.1, f32[32,4,64]{2,1,0:T(4,128)S(1)} %copy-done.6, f32[32,4,64]{2,1,0:T(4,128)S(1)} %get-tuple-element.4, f32[32,4,64]{2,1,0:T(4,128)S(1)} %bitcast.84, f32[32,4,64]{2,1,0:T(4,128)S(1)} %copy-done.8, ...), kind=kOutput, calls=%fused_computation.7 | convolution fusion | flops 8912896 | bytes 2326528 | tf_op jit(solution)/shard_map/bhvk,bhk->bhv/dot_general | solution.py:70
  55.5 2.1 fusion.28
  58.4 2.2 %convolution_convert_fusion.2 = bf16[32,2048]{1,0:T(8,128)(2,1)} fusion(bf16[32,256]{1,0:T(8,128)(2,1)S(1)} %convert_element_type.80, bf16[256,2048]{1,0:T(8,128)(2,1)} %param.35), kind=kOutput, calls=%fused_computation.16 | convolution fusion | flops 33619968 | bytes 1196032 | tf_op jit(solution)/shard_map/dot_general | solution.py:139
  71.6 34.1 %all-reduce.2.cloned.1.call-done = bf16[32,2048]{1,0:T(8,128)(2,1)} async-done(((bf16[32,2048]{1,0:T(8,128)(2,1)}), bf16[32,2048]{1,0:T(8,128)(2,1)}) %all-reduce.2.cloned.1.call-update) | async-done | bytes 131088 | tf_op jit(solution)/shard_map/psum | solution.py:140
  105.7 1.8 convert_add_fusion
  109.3 1.8 convolution_convert_fusion
  111.1 4.6 %all-to-all-start = ((bf16[8,16,2048]{2,1,0:T(8,128)(2,1)}), bf16[8,16,2048]{2,1,0:T(8,128)(2,1)}, u32[]{:S(2)}, u32[]{:S(2)}) async-start(bf16[8,16,2048]{2,1,0:T(8,128)(2,1)} %convolution_convert_fusion), calls=%async_computation | async-start | bytes 1048576 | tf_op jit(solution)/shard_map/all_to_all | solution.py:157
  115.8 15.4 %all-to-all-done = bf16[8,16,2048]{2,1,0:T(8,128)(2,1)} async-done(((bf16[8,16,2048]{2,1,0:T(8,128)(2,1)}), bf16[8,16,2048]{2,1,0:T(8,128)(2,1)}, u32[]{:S(2)}, u32[]{:S(2)}) %all-to-all-start) | async-done | bytes 524320 | tf_op jit(solution)/shard_map/all_to_all | solution.py:157
  131.2 3.9 %fusion.5 = f32[128,1024]{1,0:T(8,128)} fusion(bf16[128,2048]{1,0:T(8,128)(2,1)} %bitcast.9, bf16[1,2048,1024]{2,1,0:T(8,128)(2,1)} %param.39), kind=kOutput, calls=%fused_computation.5 | convolution fusion | flops 536870912 | bytes 5242880 | tf_op jit(solution)/shard_map/lrd,ldf->lrf/dot_general | solution.py:162
  135.0 6.0 %fusion.14 = bf16[1,128,2048]{2,1,0:T(8,128)(2,1)} fusion(bf16[1,1024,2048]{2,1,0:T(8,128)(2,1)} %param.41, bf16[128,2048]{1,0:T(8,128)(2,1)} %bitcast.9, bf16[1,2048,1024]{2,1,0:T(8,128)(2,1)} %param.40, f32[128,1024]{1,0:T(8,128)} %fusion.5), kind=kOutput, calls=%fused_computation.13 | convolution fusion | flops 1074790400 | bytes 9961472 | tf_op jit(solution)/shard_map/lrf,lfd->lrd/dot_general | solution.py:169
  142.5 4.2 %all-to-all-start.3 = ((bf16[8,8,2048]{2,1,0:T(8,128)(2,1)}), bf16[8,8,2048]{2,1,0:T(8,128)(2,1)}, u32[]{:S(2)}, u32[]{:S(2)}) async-start(bf16[8,8,2048]{2,1,0:T(8,128)(2,1)} %broadcast_in_dim.2), calls=%async_computation.4 | async-start | bytes 524288 | tf_op jit(solution)/shard_map/all_to_all | solution.py:158
  146.8 3.8 %broadcast_multiply_fusion = f32[32,4,64,64]{3,2,1,0:T(8,128)} fusion(f32[32,4,64]{2,1,0:T(4,128)} %mul.243, f32[32,4,64]{2,1,0:T(4,128)} %mul.240), kind=kLoop, calls=%fused_computation.18 | loop fusion | flops 524288 | bytes 2162688 | tf_op jit(solution)/shard_map/mul | solution.py:68
  150.6 5.1 %mul.277 = f32[32,4,4096]{2,1,0:T(4,128)} reshape(f32[32,4,64,64]{3,2,1,0:T(8,128)} %broadcast_multiply_fusion) | data formatting | bytes 4194304 | tf_op jit(solution)/shard_map/mul | solution.py:68
  155.6 3.8 %broadcast_multiply_fusion.1 = f32[32,4,64,64]{3,2,1,0:T(8,128)} fusion(f32[32,4,64]{2,1,0:T(4,128)} %copy-done.5, f32[32,4,64]{2,1,0:T(4,128)} %bitcast.85), kind=kLoop, calls=%fused_computation.19 | loop fusion | flops 524288 | bytes 2162688 | tf_op jit(solution)/shard_map/mul | solution.py:67
  159.4 5.0 %mul.276 = f32[32,4,4096]{2,1,0:T(4,128)} reshape(f32[32,4,64,64]{3,2,1,0:T(8,128)} %broadcast_multiply_fusion.1) | data formatting | bytes 4194304 | tf_op jit(solution)/shard_map/mul | solution.py:67
  164.5 3.0 %mul.227 = f32[32,4,64,64]{3,2,1,0:T(8,128)} broadcast(f32[32,4,64]{2,1,0:T(4,128)} %mul.226), dimensions={0,1,3} | broadcast | bytes 2129920 | tf_op jit(solution)/shard_map/mul | solution.py:66
  167.5 5.0 %mul.274 = f32[32,4,4096]{2,1,0:T(4,128)} reshape(f32[32,4,64,64]{3,2,1,0:T(8,128)} %mul.227) | data formatting | bytes 4194304 | tf_op jit(solution)/shard_map/mul | solution.py:66
  172.5 2.6 %fusion.44 = f32[64,352]{1,0:T(8,128)} fusion(bf16[2048,352]{0,1:T(8,128)(2,1)} %param.42, bf16[8,8,2048]{2,1,0:T(8,128)(2,1)} %all-to-all-done.3), kind=kOutput, calls=%fused_computation.46 | convolution fusion | flops 92274688 | bytes 1794048 | tf_op jit(solution)/shard_map/dot_general | solution.py:179
  175.2 4.8 %all-to-all-start.1 = ((bf16[8,16,512]{2,1,0:T(8,128)(2,1)}), bf16[8,16,512]{2,1,0:T(8,128)(2,1)}, u32[]{:S(2)}, u32[]{:S(2)}) async-start(bf16[8,16,512]{2,1,0:T(8,128)(2,1)} %bitcast.91), calls=%async_computation.2 | async-start | bytes 262144 | tf_op jit(solution)/shard_map/all_to_all | solution.py:187
  180.0 3.3 %fusion.17 = bf16[8,8,2048]{2,1,0:T(8,128)(2,1)} fusion(bf16[352,2048]{1,0:T(8,128)(2,1)S(1)} %copy-done, bf16[2048,352]{0,1:T(8,128)(2,1)} %param.43, bf16[8,8,2048]{2,1,0:T(8,128)(2,1)} %all-to-all-done.3, f32[64,352]{1,0:T(8,128)} %fusion.44), kind=kOutput, calls=%fused_computation.15 | convolution fusion | flops 184815616 | bytes 3497984 | tf_op jit(solution)/shard_map/dot_general | solution.py:182
  183.3 3.5 %all-to-all-done.1 = bf16[8,16,512]{2,1,0:T(8,128)(2,1)} async-done(((bf16[8,16,512]{2,1,0:T(8,128)(2,1)}), bf16[8,16,512]{2,1,0:T(8,128)(2,1)}, u32[]{:S(2)}, u32[]{:S(2)}) %all-to-all-start.1) | async-done | bytes 131104 | tf_op jit(solution)/shard_map/all_to_all | solution.py:187
  186.8 4.0 %all-to-all-start.4 = ((bf16[8,8,2048]{2,1,0:T(8,128)(2,1)}), bf16[8,8,2048]{2,1,0:T(8,128)(2,1)}, u32[]{:S(2)}, u32[]{:S(2)}) async-start(bf16[8,8,2048]{2,1,0:T(8,128)(2,1)} %fusion.17), calls=%async_computation.5 | async-start | bytes 524288 | tf_op jit(solution)/shard_map/all_to_all | solution.py:188
  190.9 4.7 %subtract_add_fusion = f32[16,8,4096]{2,1,0:T(8,128)} fusion(f32[16,8,4096]{2,1,0:T(8,128)} %bitcast.80, f32[16,8,4096]{2,1,0:T(8,128)} %bitcast.81, f32[16,8,4096]{2,1,0:T(8,128)S(1)} %bitcast.79, f32[16,8,4096]{2,1,0:T(8,128)} %bitcast.82), kind=kLoop, calls=%fused_computation.17 | loop fusion | flops 1572864 | bytes 10485760 | tf_op jit(solution)/shard_map/add | solution.py:66
  197.4 3.2 %all-to-all-done.4 = bf16[8,8,2048]{2,1,0:T(8,128)(2,1)} async-done(((bf16[8,8,2048]{2,1,0:T(8,128)(2,1)}), bf16[8,8,2048]{2,1,0:T(8,128)(2,1)}, u32[]{:S(2)}, u32[]{:S(2)}) %all-to-all-start.4) | async-done | bytes 262176 | tf_op jit(solution)/shard_map/all_to_all | solution.py:188
  200.6 3.3 %all-to-all-start.2 = ((f32[4,8,512]{2,1,0:T(8,128)}), f32[4,8,512]{2,1,0:T(8,128)S(1)}, u32[]{:S(2)}, u32[]{:S(2)}) async-start(f32[4,8,512]{2,1,0:T(8,128)} %convolution_bitcast_fusion), calls=%async_computation.3 | async-start | bytes 131072 | tf_op jit(solution)/shard_map/all_to_all | solution.py:195
  204.9 3.8 %all-to-all-done.2 = f32[4,8,512]{2,1,0:T(8,128)S(1)} async-done(((f32[4,8,512]{2,1,0:T(8,128)}), f32[4,8,512]{2,1,0:T(8,128)S(1)}, u32[]{:S(2)}, u32[]{:S(2)}) %all-to-all-start.2) | async-done | bytes 65568 | tf_op jit(solution)/shard_map/all_to_all | solution.py:195
  (72 shorter events, 37.7 us)
Async XLA Ops:
  7.2 172.8 %copy-start = (bf16[352,2048]{1,0:T(8,128)(2,1)S(1)}, bf16[352,2048]{1,0:T(8,128)(2,1)}, u32[]{:S(2)}) copy-start(bf16[352,2048]{1,0:T(8,128)(2,1)} %param.44) | copy-start | bytes 4325380
  7.2 16.7 %copy-start.10 = (f32[2048]{0:T(1024)S(1)}, f32[2048]{0:T(1024)}, u32[]{:S(2)}) copy-start(f32[2048]{0:T(1024)} %param.25) | copy-start | bytes 24580
  7.2 16.7 %copy-start.13 = (f32[256]{0:T(256)S(1)}, f32[256]{0:T(256)}, u32[]{:S(2)}) copy-start(f32[256]{0:T(256)} %param.32) | copy-start | bytes 3076
  7.2 24.2 %copy-start.2 = (f32[32,4,4096]{2,1,0:T(4,128)S(1)}, f32[32,4,4096]{2,1,0:T(4,128)}, u32[]{:S(2)}) copy-start(f32[32,4,4096]{2,1,0:T(4,128)} %param.24) | copy-start | bytes 6291460
  7.2 98.5 %all-reduce.2.cloned.1.call-start = ((), (), s32[]{:S(2)}) async-start(), calls=%async_computation.6 | async-start | bytes 262144 | tf_op jit(solution)/shard_map/psum | solution.py:140
  34.7 9.7 %copy-start.1 = (f32[32,4,64,64]{3,2,1,0:T(8,128)S(1)}, f32[32,4,64,64]{3,2,1,0:T(8,128)}, u32[]{:S(2)}) copy-start(f32[32,4,64,64]{3,2,1,0:T(8,128)} %reshape.173) | copy-start | bytes 6291460
  34.7 9.8 %copy-start.6 = (f32[32,4,64]{2,1,0:T(4,128)S(1)}, f32[32,4,64]{2,1,0:T(4,128)}, u32[]{:S(2)}) copy-start(f32[32,4,64]{2,1,0:T(4,128)} %mul.226) | copy-start | bytes 98308
  34.7 9.8 %copy-start.7 = (f32[32,4,64]{2,1,0:T(4,128)S(1)}, f32[32,4,64]{2,1,0:T(4,128)}, u32[]{:S(2)}) copy-start(f32[32,4,64]{2,1,0:T(4,128)} %mul.240) | copy-start | bytes 98308
  34.7 9.8 %copy-start.8 = (f32[32,4,64]{2,1,0:T(4,128)S(1)}, f32[32,4,64]{2,1,0:T(4,128)}, u32[]{:S(2)}) copy-start(f32[32,4,64]{2,1,0:T(4,128)} %mul.243) | copy-start | bytes 98308
  34.7 9.8 %copy-start.11 = (f32[32,4,64,1]{2,1,0,3:T(4,128)S(1)}, f32[32,4,64,1]{2,1,0,3:T(4,128)}, u32[]{:S(2)}) copy-start(f32[32,4,64,1]{2,1,0,3:T(4,128)} %reshape.185) | copy-start | bytes 98308
  35.9 17.6 %copy-start.5 = (f32[32,4,64]{2,1,0:T(4,128)}, f32[32,4,64]{2,1,0:T(4,128)S(1)}, u32[]{:S(2)}) copy-start(f32[32,4,64]{2,1,0:T(4,128)S(1)} %get-tuple-element.4) | copy-start | bytes 98308
  44.5 9.0 %copy-start.4 = (f32[32,4,1,64]{3,2,1,0:T(1,128)}, f32[32,4,1,64]{3,2,1,0:T(1,128)S(1)}, u32[]{:S(2)}) copy-start(f32[32,4,1,64]{3,2,1,0:T(1,128)S(1)} %fusion.70) | copy-start | bytes 98308
  108.6 0.7 copy-start.3
  111.1 20.0 %all-to-all-start = ((bf16[8,16,2048]{2,1,0:T(8,128)(2,1)}), bf16[8,16,2048]{2,1,0:T(8,128)(2,1)}, u32[]{:S(2)}, u32[]{:S(2)}) async-start(bf16[8,16,2048]{2,1,0:T(8,128)(2,1)} %convolution_convert_fusion), calls=%async_computation | async-start | bytes 1048576 | tf_op jit(solution)/shard_map/all_to_all | solution.py:157
  115.7 59.4 %reduce-scatter.2.cloned.1.call-start = ((), (), s32[]{:S(2)}) async-start(), calls=%async_computation.7 | async-start | bytes 655360 | tf_op jit(solution)/shard_map/reduce_scatter | solution.py:172
  142.5 30.0 %all-to-all-start.3 = ((bf16[8,8,2048]{2,1,0:T(8,128)(2,1)}), bf16[8,8,2048]{2,1,0:T(8,128)(2,1)}, u32[]{:S(2)}, u32[]{:S(2)}) async-start(bf16[8,8,2048]{2,1,0:T(8,128)(2,1)} %broadcast_in_dim.2), calls=%async_computation.4 | async-start | bytes 524288 | tf_op jit(solution)/shard_map/all_to_all | solution.py:158
  175.2 11.7 %all-to-all-start.1 = ((bf16[8,16,512]{2,1,0:T(8,128)(2,1)}), bf16[8,16,512]{2,1,0:T(8,128)(2,1)}, u32[]{:S(2)}, u32[]{:S(2)}) async-start(bf16[8,16,512]{2,1,0:T(8,128)(2,1)} %bitcast.91), calls=%async_computation.2 | async-start | bytes 262144 | tf_op jit(solution)/shard_map/all_to_all | solution.py:187
  186.8 13.8 %all-to-all-start.4 = ((bf16[8,8,2048]{2,1,0:T(8,128)(2,1)}), bf16[8,8,2048]{2,1,0:T(8,128)(2,1)}, u32[]{:S(2)}, u32[]{:S(2)}) async-start(bf16[8,8,2048]{2,1,0:T(8,128)(2,1)} %fusion.17), calls=%async_computation.5 | async-start | bytes 524288 | tf_op jit(solution)/shard_map/all_to_all | solution.py:188
  190.9 4.8 %copy-start.12 = (f32[2048]{0:T(1024)S(1)}, f32[2048]{0:T(1024)}, u32[]{:S(2)}) copy-start(f32[2048]{0:T(1024)} %param.45) | copy-start | bytes 24580
  190.9 4.8 %copy-start.9 = (f32[32,8,16]{0,2,1:T(8,128)S(1)}, f32[32,8,16]{0,2,1:T(8,128)}, u32[]{:S(2)}) copy-start(f32[32,8,16]{0,2,1:T(8,128)} %get-tuple-element.2) | copy-start | bytes 49156
  200.6 8.1 %all-to-all-start.2 = ((f32[4,8,512]{2,1,0:T(8,128)}), f32[4,8,512]{2,1,0:T(8,128)S(1)}, u32[]{:S(2)}, u32[]{:S(2)}) async-start(f32[4,8,512]{2,1,0:T(8,128)} %convolution_bitcast_fusion), calls=%async_computation.3 | async-start | bytes 131072 | tf_op jit(solution)/shard_map/all_to_all | solution.py:195
Sparse Core Ops, SparseCore 0:
  60.7 44.9 all-reduce.1
  141.2 23.0 reduce-scatter.1
where the time goes:
time: 219 us; the launch traced here: 217 us
  waiting for transfers between devices  60.1 us (27%)
  matrix products  48.1 us (22%)
  local copies, waits for them, and re-layouts  41.5 us (19%)
  other arithmetic  32 us (15%)
  starting transfers between devices  21 us (10%)
  between operations  14.3 us (7%)
    psum x1, waiting for transfers between devices, local(): lax.psum(partial_out.astype(jnp.bfloat16), 'tp').astype(jnp.float32)  34.1 us
    all_to_all x1, waiting for transfers between devices, local(): lax.all_to_all(send_rows, 'ep', split_axis=0, concat_axis=0, tiled=True)  15.4 us
    mul x3, local copies, waits for them, and re-layouts, state_update(): matrix * decay_head[:, :, None, :]  9.51 us
    dot_general x1, matrix products, state_update(): jnp.einsum('bhvk,bhk->bhv', updated, head_receptance, precision=PRECISE)  8.96 us
    dot_general x1, matrix products, state_update(): removed = jnp.einsum('bhvk,bhk->bhv', matrix, unit_keys, precision=PRECISE)  8.58 us
    mul x3, local copies, waits for them, and re-layouts, state_update(): head_values[..., None] * head_keys[:, :, None, :]  7.99 us
    dot_general x1, matrix products, local(): jnp.einsum('lrf,lfd->lrd', expert_hidden, expert_down_weight, preferred_e...  5.98 us
    reshape x4, local copies, waits for them, and re-layouts, split_heads(): return block.reshape(seq_count, -1, head_width)  5.88 us
  transfers between devices with their start and end apart: 7, of which 5 were waited for; matrix products, arithmetic and copies ran while one was open for 24% of the time, Pallas kernels for 0%

commit v1 on v0

--- a/solution.py
+++ b/solution.py
@@ -1,6 +1,10 @@
+import functools
+
 import jax
 import jax.numpy as jnp
 from jax import lax
+from jax.experimental import pallas as pl
+from jax.experimental.pallas import tpu as pltpu
 from jax.sharding import PartitionSpec as P
 
 HEAD_WIDTH = 64
@@ -200,9 +204,382 @@
     return (layer_out, next_state)
 
 
+def proj_state_kernel(
+    tokens_ref, gain_ref, wr_ref, wk_ref, wv_ref, wd_ref, doff_ref, coff_ref, cfac_ref,
+    own_ref, hgain_ref, wo_ref, routes_ref, rweight_ref, state_ref,
+    next_ref, part_ref, base_ref, wext_ref,
+    sbuf, nbuf, in_sem, out_sem,
+):
+    seqs, width = tokens_ref.shape
+    heads = state_ref.shape[1]
+    lanes = part_ref.shape[0]
+    rows = part_ref.shape[1]
+    loads = [
+        pltpu.make_async_copy(state_ref.at[:, h, :], sbuf.at[h], in_sem.at[h]) for h in range(heads)
+    ]
+    for load in loads:
+        load.start()
+    f32, bf16 = jnp.float32, jnp.bfloat16
+    toks = tokens_ref[...].astype(f32)
+    normed = (
+        toks * lax.rsqrt(jnp.mean(toks * toks, axis=-1, keepdims=True) + 1e-06) * gain_ref[...]
+    ).astype(bf16)
+    recept = jnp.dot(normed, wr_ref[...], preferred_element_type=f32)
+    keys = jnp.dot(normed, wk_ref[...], preferred_element_type=f32)
+    values = jnp.dot(normed, wv_ref[...], preferred_element_type=f32)
+    logits = jnp.dot(normed, wd_ref[...], preferred_element_type=f32)
+    decay = jnp.exp(-jnp.exp(doff_ref[...] + logits))
+    rate = jax.nn.sigmoid(coff_ref[...] + cfac_ref[...] * keys)
+    key_in = keys * rate
+    own_prod = recept * key_in * own_ref[...]
+    hgain = jnp.broadcast_to(hgain_ref[...], keys.shape)
+    pair = 2 * HEAD_WIDTH
+    lane = lax.broadcasted_iota(jnp.int32, (seqs, pair), 1)
+    low = lane < HEAD_WIDTH
+    half_r = lax.broadcasted_iota(jnp.int32, (pair, pair), 0) // HEAD_WIDTH
+    half_c = lax.broadcasted_iota(jnp.int32, (pair, pair), 1) // HEAD_WIDTH
+    ones_block = (half_r == half_c).astype(f32).astype(bf16)
+
+    def group_sum(block):
+        high = block.astype(bf16)
+        rest = (block - high.astype(f32)).astype(bf16)
+        return jnp.dot(high, ones_block, preferred_element_type=f32) + jnp.dot(
+            rest, ones_block, preferred_element_type=f32
+        )
+
+    def doubled(full, h):
+        chunk = full[:, (h // 2) * pair : (h // 2 + 1) * pair]
+        turned = pltpu.roll(chunk, HEAD_WIDTH, 1)
+        return jnp.where(low, chunk, turned) if h % 2 == 0 else jnp.where(low, turned, chunk)
+
+    chunks = state_ref.shape[2] // pair
+    step = 8
+    outs, stores = [], []
+    for h in range(heads):
+        k2, r2, v2 = doubled(keys, h), doubled(recept, h), doubled(values, h)
+        d2, kin2, rate2 = doubled(decay, h), doubled(key_in, h), doubled(rate, h)
+        unit = (
+            k2
+            * lax.rsqrt(jnp.mean(k2 * k2, axis=-1, keepdims=True) + 1e-06)
+            * HEAD_WIDTH ** (-0.5)
+        )
+        own_total = 0.5 * jnp.sum(doubled(own_prod, h), axis=-1, keepdims=True)
+
+        def many(block):
+            return jnp.concatenate([block] * step, axis=0)
+
+        unit_m, back_m, dec_m = many(unit), many(unit * rate2), many(d2)
+        kin_m, rec_m = many(kin2), many(r2)
+        loads[h].wait()
+        acc = jnp.zeros((seqs, pair), f32)
+        for q in range(0, chunks, step):
+            picks = [(lane == 2 * j) | (lane == HEAD_WIDTH + 2 * j + 1) for j in range(q, q + step)]
+            old = jnp.concatenate(
+                [sbuf[h, :, j * pair : (j + 1) * pair] for j in range(q, q + step)], axis=0
+            )
+            removed = group_sum(old * unit_m)
+            spread_v = group_sum(jnp.concatenate([jnp.where(p, v2, 0.0) for p in picks], axis=0))
+            new = old * dec_m - removed * back_m + spread_v * kin_m
+            for i in range(step):
+                nbuf[h, :, (q + i) * pair : (q + i + 1) * pair] = new[i * seqs : (i + 1) * seqs]
+            read = group_sum(new * rec_m)
+            for i in range(step):
+                acc = acc + jnp.where(picks[i], read[i * seqs : (i + 1) * seqs], 0.0)
+        store = pltpu.make_async_copy(nbuf.at[h], next_ref.at[:, h, :], out_sem.at[h])
+        store.start()
+        stores.append(store)
+        y = acc + pltpu.roll(acc, HEAD_WIDTH, 1)
+        center = y - jnp.mean(y, axis=-1, keepdims=True)
+        var = jnp.mean(center * center, axis=-1, keepdims=True)
+        outs.append(center * lax.rsqrt(var + 0.00064) * doubled(hgain, h) + own_total * v2)
+    merged = jnp.concatenate(
+        [jnp.where(low, outs[h], outs[h + 1]) for h in range(0, heads, 2)], axis=1
+    ).astype(bf16)
+    part = jnp.dot(merged, wo_ref[...], preferred_element_type=f32)
+    me_lane = lax.axis_index("tp")
+    base = jnp.zeros((rows, width), f32)
+    for i in range(lanes):
+        mine = part[i * rows : (i + 1) * rows]
+        part_ref[i] = mine.astype(bf16)
+        base = jnp.where(me_lane == i, mine + toks[i * rows : (i + 1) * rows], base)
+    base_ref[...] = base
+    start = pl.multiple_of(lax.axis_index("ep") * seqs + me_lane * rows, 8)
+    own_start = pl.multiple_of(me_lane * rows, 8)
+    routes = routes_ref[pl.ds(start, rows), :]
+    weights = rweight_ref[pl.ds(own_start, rows), :]
+    column = lax.broadcasted_iota(jnp.int32, (rows, 128), 1) % 64
+    table = jnp.zeros((rows, 128), f32)
+    for k in range(routes.shape[1]):
+        table = table + jnp.where(column == routes[:, k : k + 1], weights[:, k : k + 1], 0.0)
+    wext_ref[...] = table
+    for store in stores:
+        store.wait()
+
+
+def exchange_kernel(
+    groups, lanes,
+    part_ref, base_ref, wext_ref, gain_ref, goff_ref,
+    eg_hbm, eu_hbm, ed_hbm, dg_hbm, du_hbm, dd_hbm,
+    out_ref,
+    eg, eu, ed, dg, du, dd, p_in, xs, flat, hid, dens, ys, y_in, z_in, v_out, v_in,
+    w_sem, s1, r1, sz, rz, st, rt, sc, rc, sa, ra, sb, rb, sv, rv,
+):
+    f32, bf16 = jnp.float32, jnp.bfloat16
+    rows, width = base_ref.shape
+    zs = groups // 2
+    me_g, me_l = lax.axis_index("ep"), lax.axis_index("tp")
+    core, me_z = lax.rem(me_g, 2), me_g // 2
+    partner = (me_g + 1 - 2 * core, me_l)
+
+    def lane_peer(d):
+        return (me_g, lax.rem(me_l + d + lanes, lanes))
+
+    def z_peer(d):
+        return (lax.rem(me_z + d + zs, zs) * 2 + core, me_l)
+
+    def send(src, dst, ssem, rsem, peer):
+        copy = pltpu.make_async_remote_copy(
+            src_ref=src, dst_ref=dst, send_sem=ssem, recv_sem=rsem, device_id=peer,
+            device_id_type=pl.DeviceIdType.MESH,
+        )
+        copy.start()
+        return copy
+
+    pulls = [
+        pltpu.make_async_copy(src, dst, w_sem.at[i])
+        for i, (src, dst) in enumerate(
+            [(dg_hbm, dg), (du_hbm, du), (dd_hbm, dd), (eg_hbm.at[0], eg), (eu_hbm.at[0], eu),
+             (ed_hbm.at[0], ed)]
+        )
+    ]
+    for pull in pulls:
+        pull.start()
+    barrier = pltpu.get_barrier_semaphore()
+    peers = [lane_peer(d) for d in range(1, lanes)] + [z_peer(d) for d in range(1, zs)] + [partner]
+    for peer in peers:
+        pl.semaphore_signal(barrier, inc=1, device_id=peer, device_id_type=pl.DeviceIdType.MESH)
+    pl.semaphore_wait(barrier, len(peers))
+    sent = []
+    firsts = []
+    for d in range(1, lanes):
+        target = lax.rem(me_l + lanes - d, lanes)
+        firsts.append(
+            send(part_ref.at[target], p_in.at[d - 1], s1.at[d - 1], r1.at[d - 1], (me_g, target))
+        )
+    hidden = base_ref[...]
+    for d, copy in enumerate(firsts):
+        copy.wait_recv()
+        hidden = hidden + p_in[d].astype(f32)
+    sent += firsts
+    normed = hidden * lax.rsqrt(jnp.mean(hidden * hidden, axis=-1, keepdims=True) + 1e-06)
+    xs[0, 0, 0, :, :width] = (normed * gain_ref[...]).astype(bf16)
+    table = wext_ref[...]
+    high = table.astype(bf16).astype(f32)
+    first_half = lax.broadcasted_iota(jnp.int32, table.shape, 1) < 64
+    xs[0, 0, 0, :, width:] = jnp.where(first_half, high, table - high).astype(bf16)
+    hold_z, hold_t, hold_c = {}, {}, {}
+    for d in range(1, zs):
+        hold_z[d] = send(xs.at[0, 0, 0], xs.at[0, 0, d], sz.at[d - 1], rz.at[d - 1], z_peer(d))
+
+    def to_partner(d, q):
+        i = d * zs + q
+        hold_c[d, q] = send(xs.at[0, d, q], xs.at[1, d, q], sc.at[i], rc.at[i], partner)
+
+    def to_lanes(q):
+        to_partner(0, q)
+        for d in range(1, lanes):
+            i = (d - 1) * zs + q
+            hold_t[d, q] = send(xs.at[0, 0, q], xs.at[0, d, q], st.at[i], rt.at[i], lane_peer(d))
+
+    to_lanes(0)
+    for q in range(1, zs):
+        hold_z[q].wait_recv()
+        to_lanes(q)
+    block = 2 * zs * rows
+
+    def gathered(d):
+        return xs[:, d].astype(f32).reshape(block, width + 128)
+
+    for q in range(zs):
+        hold_c[0, q].wait_recv()
+    mine = gathered(0)
+    flat[0:block] = mine.astype(bf16)
+    own_rows = mine[:, :width].astype(bf16)
+    for pull in pulls[:3]:
+        pull.wait()
+    gate = jnp.dot(own_rows, dg[...], preferred_element_type=f32)
+    up = jnp.dot(own_rows, du[...], preferred_element_type=f32)
+    mixed = (jax.nn.silu(gate) * up).astype(bf16)
+    dens[...] = jnp.dot(mixed, dd[...], preferred_element_type=f32) * jax.nn.sigmoid(goff_ref[...])
+    for q in range(zs):
+        for d in range(1, lanes):
+            hold_t[d, q].wait_recv()
+            to_partner(d, q)
+    for d in range(1, lanes):
+        for q in range(zs):
+            hold_c[d, q].wait_recv()
+        flat[d * block : (d + 1) * block] = gathered(d).astype(bf16)
+    for pull in pulls[3:]:
+        pull.wait()
+    tile = 256
+
+    @pl.loop(0, eg.shape[1] // tile)
+    def _(n):
+        cols = pl.ds(pl.multiple_of(n * tile, tile), tile)
+        left = flat[:, :width]
+        gated = jnp.dot(left, eg[:, cols], preferred_element_type=f32)
+        raised = jnp.dot(left, eu[:, cols], preferred_element_type=f32)
+        hid[:, cols] = (jax.nn.silu(gated) * raised).astype(bf16)
+
+    tail = flat[:, width:].astype(f32)
+    picked = lax.broadcasted_iota(jnp.int32, tail.shape, 1) % 64 == me_g
+    scale = jnp.sum(jnp.where(picked, tail, 0.0), axis=-1, keepdims=True)
+    wide = 256
+
+    @pl.loop(0, width // wide)
+    def _(n):
+        cols = pl.ds(pl.multiple_of(n * wide, wide), wide)
+        made = jnp.dot(hid[...], ed[:, cols], preferred_element_type=f32) * scale
+        for d in range(lanes):
+            piece = made[d * block : (d + 1) * block]
+            if d == 0:
+                piece = piece + dens[:, cols]
+            ys[:, d, :, :, cols] = piece.reshape(2, zs, rows, wide).astype(bf16)
+
+    to_core = [
+        send(ys.at[1, d], y_in.at[d], sa.at[d], ra.at[d], partner)
+        for d in list(range(1, lanes)) + [0]
+    ]
+    to_lane = []
+    for d in range(1, lanes):
+        to_core[d - 1].wait_recv()
+        ys[0, d] = (ys[0, d].astype(f32) + y_in[d].astype(f32)).astype(bf16)
+        to_lane.append(
+            send(ys.at[0, d], z_in.at[d - 1], sb.at[d - 1], rb.at[d - 1], lane_peer(-d))
+        )
+    to_core[lanes - 1].wait_recv()
+    total = ys[0, 0].astype(f32) + y_in[0].astype(f32)
+    for d in range(1, lanes):
+        to_lane[d - 1].wait_recv()
+        total = total + z_in[d - 1].astype(f32)
+    v_out[...] = total.astype(bf16)
+    to_z = [
+        send(v_out.at[d], v_in.at[d - 1], sv.at[d - 1], rv.at[d - 1], z_peer(-d))
+        for d in range(1, zs)
+    ]
+    result = hidden + total[0]
+    for d, copy in enumerate(to_z):
+        copy.wait_recv()
+        result = result + v_in[d].astype(f32)
+    out_ref[...] = result.astype(bf16)
+    sent += list(hold_z.values()) + list(hold_t.values()) + list(hold_c.values())
+    sent += to_core + to_lane + to_z
+    for copy in sent:
+        copy.wait_send()
+
+
+def fused(
+    tokens, recurrent_head_state, first_norm_gain, receptance_matrix, key_matrix, value_matrix,
+    decay_matrix, decay_offset, correction_offset, correction_key_factor, own_term_weight,
+    head_norm_gain, output_matrix, second_norm_gain, routing, routing_weight, expert_gate_weight,
+    expert_up_weight, expert_down_weight, dense_gate_weight, dense_up_weight, dense_down_weight,
+    dense_gate_offset,
+):
+    f32, bf16 = jnp.float32, jnp.bfloat16
+    seqs, width = tokens.shape
+    heads, flat_width = recurrent_head_state.shape[1:]
+    groups, lanes = lax.axis_size("ep"), lax.axis_size("tp")
+    rows, zs = seqs // lanes, groups // 2
+    vmem = pl.BlockSpec(memory_space=pltpu.VMEM)
+    anywhere = pl.BlockSpec(memory_space=pl.ANY)
+    dma = pltpu.SemaphoreType.DMA
+
+    def row(vector):
+        return vector.reshape(1, -1)
+
+    next_state, part, base, table = pl.pallas_call(
+        proj_state_kernel,
+        out_shape=(
+            jax.ShapeDtypeStruct(recurrent_head_state.shape, f32),
+            jax.ShapeDtypeStruct((lanes, rows, width), bf16),
+            jax.ShapeDtypeStruct((rows, width), f32),
+            jax.ShapeDtypeStruct((rows, 128), f32),
+        ),
+        in_specs=[vmem] * 14 + [anywhere],
+        out_specs=(anywhere, vmem, vmem, vmem),
+        scratch_shapes=[
+            pltpu.VMEM((heads, seqs, flat_width), f32),
+            pltpu.VMEM((heads, seqs, flat_width), f32),
+            dma((heads,)),
+            dma((heads,)),
+        ],
+        compiler_params=pltpu.CompilerParams(vmem_limit_bytes=40 * 1024 * 1024),
+        name="proj_state",
+    )(
+        tokens, row(first_norm_gain), receptance_matrix, key_matrix, value_matrix, decay_matrix,
+        row(decay_offset), row(correction_offset), row(correction_key_factor),
+        row(own_term_weight), row(head_norm_gain), output_matrix, routing, routing_weight,
+        recurrent_head_state,
+    )
+    hidden_units = expert_gate_weight.shape[2]
+    total = groups * seqs
+    layer_out = pl.pallas_call(
+        functools.partial(exchange_kernel, groups, lanes),
+        out_shape=jax.ShapeDtypeStruct((rows, width), bf16),
+        in_specs=[vmem] * 5 + [anywhere] * 6,
+        out_specs=vmem,
+        scratch_shapes=[
+            pltpu.VMEM(expert_gate_weight.shape[1:], bf16),
+            pltpu.VMEM(expert_up_weight.shape[1:], bf16),
+            pltpu.VMEM(expert_down_weight.shape[1:], bf16),
+            pltpu.VMEM(dense_gate_weight.shape, bf16),
+            pltpu.VMEM(dense_up_weight.shape, bf16),
+            pltpu.VMEM(dense_down_weight.shape, bf16),
+            pltpu.VMEM((lanes - 1, rows, width), bf16),
+            pltpu.VMEM((2, lanes, zs, rows, width + 128), bf16),
+            pltpu.VMEM((total, width + 128), bf16),
+            pltpu.VMEM((total, hidden_units), bf16),
+            pltpu.VMEM((2 * zs * rows, width), f32),
+            pltpu.VMEM((2, lanes, zs, rows, width), bf16),
+            pltpu.VMEM((lanes, zs, rows, width), bf16),
+            pltpu.VMEM((lanes - 1, zs, rows, width), bf16),
+            pltpu.VMEM((zs, rows, width), bf16),
+            pltpu.VMEM((zs - 1, rows, width), bf16),
+            dma((6,)),
+            dma((lanes - 1,)), dma((lanes - 1,)),
+            dma((zs - 1,)), dma((zs - 1,)),
+            dma(((lanes - 1) * zs,)), dma(((lanes - 1) * zs,)),
+            dma((lanes * zs,)), dma((lanes * zs,)),
+            dma((lanes,)), dma((lanes,)),
+            dma((lanes - 1,)), dma((lanes - 1,)),
+            dma((zs - 1,)), dma((zs - 1,)),
+        ],
+        compiler_params=pltpu.CompilerParams(
+            collective_id=0, has_side_effects=True, vmem_limit_bytes=48 * 1024 * 1024
+        ),
+        name="exchange",
+    )(
+        part, base, table, row(second_norm_gain), row(dense_gate_offset), expert_gate_weight,
+        expert_up_weight, expert_down_weight, dense_gate_weight, dense_up_weight,
+        dense_down_weight,
+    )
+    return (layer_out, next_state)
+
+
+def choose(tokens, recurrent_head_state, *rest):
+    groups, lanes = lax.axis_size("ep"), lax.axis_size("tp")
+    rows, heads = tokens.shape[0] // lanes, recurrent_head_state.shape[1]
+    experts_here = rest[14].shape[0]
+    fits = (
+        rows % 8 == 0 and heads % 2 == 0 and groups % 2 == 0 and groups > 2 and lanes > 1
+        and groups <= 64 and experts_here == 1
+    )
+    return (fused if fits else local)(tokens, recurrent_head_state, *rest)
+
+
 def solution(mesh):
     return jax.shard_map(
-        local,
+        choose,
         mesh=mesh,
         in_specs=(
             P("ep", None),

time: 219 us -> 67.8 us (0.31)
  waiting for transfers between devices: 60.1 us -> 0 us
  matrix products: 48.1 us -> 0 us
  Pallas kernels: 0 us -> 47.5 us
  other arithmetic: 32 us -> 0 us
  local copies, waits for them, and re-layouts: 41.5 us -> 19 us
  starting transfers between devices: 21 us -> 0 us
  between operations: 14.3 us -> 0.73 us
    dot_general x13 -> x0, matrix products: 48.1 us -> none  [the longest x1 8.96 us: state_update(): jnp.einsum('bhvk,bhk->bhv', updated, head_receptance, precision=PRECISE)]
    pallas_call x0 -> x2, Pallas kernels: none -> 47.5 us  [the longest x1 39.2 us: fused(): pl.pallas_call(functools.partial(exchange_kernel, groups, lanes), out_sha...]
    psum x1 -> x0, waiting for transfers between devices: 34.1 us -> none  [local(): lax.psum(partial_out.astype(jnp.bfloat16), 'tp').astype(jnp.float32)]
    all_to_all x5 -> x0, waiting for transfers between devices: 25.9 us -> none  [the longest x1 15.4 us: local(): lax.all_to_all(send_rows, 'ep', split_axis=0, concat_axis=0, tiled=True)]
    mul x9 -> x0, local copies, waits for them, and re-layouts: 25.2 us -> none  [the longest x3 9.51 us: state_update(): matrix * decay_head[:, :, None, :]]
    all_to_all x5 -> x0, starting transfers between devices: 21 us -> none  [the longest x1 4.82 us: local(): lax.all_to_all(back_send, 'ep', split_axis=0, concat_axis=0, tiled=True)]
    unnamed x28 -> x39, local copies, waits for them, and re-layouts: 0.71 us -> 19 us
    mul x4 -> x0, other arithmetic: 10.8 us -> none  [the longest x1 3.82 us: state_update(): head_values[..., None] * head_keys[:, :, None, :]]
  transfers between devices with their start and end apart: 7 -> 0, of which waited for: 5 -> 0; matrix products, arithmetic and copies ran while one was open for 24% -> 0% of each run, Pallas kernels for 0% -> 0%
where the time goes in v1:
time: 67.8 us; the launch traced here: 67.2 us
  Pallas kernels  47.5 us (70%)
  local copies, waits for them, and re-layouts  19 us (28%)
  between operations  0.73 us (1%)
    pallas_call x1, Pallas kernels, fused(): pl.pallas_call(functools.partial(exchange_kernel, groups, lanes), out_sha...  39.2 us
    unnamed x39, local copies, waits for them, and re-layouts  19 us
    pallas_call x1, Pallas kernels, fused(): pl.pallas_call(proj_state_kernel, out_shape=(jax.ShapeDtypeStruct(recurre...  8.35 us

profile of v1, /device:TPU:0, one launch (start us, length us, event | category | flops | bytes accessed | tf_op | source)
XLA Modules:
  0.0 67.2 jit_solution(12351191739388749808)
XLA Ops:
  0.6 0.8 %copy.25.routes_ref = s32[256,2]{1,0:T(8,128)S(1)} copy(s32[256,2]{0,1:T(2,128)} %param.37) | data formatting | bytes 4096 | tf_op args[14]
  1.4 0.8 %copy.26.rweight_ref = f32[32,2]{1,0:T(8,128)S(1)} copy(f32[32,2]{0,1:T(2,128)} %param.38) | data formatting | bytes 512 | tf_op args[15]
  2.2 0.0 copy-start
  2.2 1.6 %copy-done = f32[32,4,4096]{2,1,0:T(4,128)S(1)} copy-done((f32[32,4,4096]{2,1,0:T(4,128)S(1)}, f32[32,4,4096]{2,1,0:T(4,128)}, u32[]{:S(2)}) %copy-start) | copy-done | bytes 2097176
  3.8 0.0 copy-start.2
  3.8 1.2 %copy-done.2 = bf16[2048,256]{1,0:T(8,128)(2,1)S(1)} copy-done((bf16[2048,256]{1,0:T(8,128)(2,1)S(1)}, bf16[2048,256]{1,0:T(8,128)(2,1)}, u32[]{:S(2)}) %copy-start.2) | copy-done | bytes 1048600
  5.0 0.0 copy-start.3
  5.0 1.2 %copy-done.3 = bf16[2048,256]{1,0:T(8,128)(2,1)S(1)} copy-done((bf16[2048,256]{1,0:T(8,128)(2,1)S(1)}, bf16[2048,256]{1,0:T(8,128)(2,1)}, u32[]{:S(2)}) %copy-start.3) | copy-done | bytes 1048600
  6.3 0.0 copy-start.4
  6.3 1.2 %copy-done.4 = bf16[2048,256]{1,0:T(8,128)(2,1)S(1)} copy-done((bf16[2048,256]{1,0:T(8,128)(2,1)S(1)}, bf16[2048,256]{1,0:T(8,128)(2,1)}, u32[]{:S(2)}) %copy-start.4) | copy-done | bytes 1048600
  7.5 0.0 copy-start.5
  7.5 1.2 %copy-done.5 = bf16[2048,256]{1,0:T(8,128)(2,1)S(1)} copy-done((bf16[2048,256]{1,0:T(8,128)(2,1)S(1)}, bf16[2048,256]{1,0:T(8,128)(2,1)}, u32[]{:S(2)}) %copy-start.5) | copy-done | bytes 1048600
  8.7 1.2 %copy-done.6 = bf16[256,2048]{1,0:T(8,128)(2,1)S(1)} copy-done((bf16[256,2048]{1,0:T(8,128)(2,1)S(1)}, bf16[256,2048]{1,0:T(8,128)(2,1)}, u32[]{:S(2)}) %copy-start.6) | copy-done | bytes 1048600
  9.9 0.9 %copy-done.7 = bf16[32,2048]{1,0:T(8,128)(2,1)S(1)} copy-done((bf16[32,2048]{1,0:T(8,128)(2,1)S(1)}, bf16[32,2048]{1,0:T(8,128)(2,1)}, u32[]{:S(2)}) %copy-start.7) | copy-done | bytes 131096
  10.8 0.7 %copy-done.10 = f32[2048]{0:T(1024)S(1)} copy-done((f32[2048]{0:T(1024)S(1)}, f32[2048]{0:T(1024)}, u32[]{:S(2)}) %copy-start.10) | copy-done | bytes 8216
  11.5 0.7 %copy-done.11 = f32[256]{0:T(256)S(1)} copy-done((f32[256]{0:T(256)S(1)}, f32[256]{0:T(256)}, u32[]{:S(2)}) %copy-start.11) | copy-done | bytes 1048
  12.2 0.7 %copy-done.12 = f32[256]{0:T(256)S(1)} copy-done((f32[256]{0:T(256)S(1)}, f32[256]{0:T(256)}, u32[]{:S(2)}) %copy-start.12) | copy-done | bytes 1048
  12.9 0.7 %copy-done.13 = f32[256]{0:T(256)S(1)} copy-done((f32[256]{0:T(256)S(1)}, f32[256]{0:T(256)}, u32[]{:S(2)}) %copy-start.13) | copy-done | bytes 1048
  13.6 0.7 %copy-done.14 = f32[256]{0:T(256)S(1)} copy-done((f32[256]{0:T(256)S(1)}, f32[256]{0:T(256)}, u32[]{:S(2)}) %copy-start.14) | copy-done | bytes 1048
  14.3 0.7 %copy-done.15 = f32[256]{0:T(256)S(1)} copy-done((f32[256]{0:T(256)S(1)}, f32[256]{0:T(256)}, u32[]{:S(2)}) %copy-start.15) | copy-done | bytes 1048
  14.9 8.3 %proj_state.1 = (f32[32,4,4096]{2,1,0:T(4,128)}, bf16[4,8,2048]{2,1,0:T(8,128)(2,1)S(1)}, f32[8,2048]{1,0:T(8,128)S(1)}, f32[8,128]{1,0:T(8,128)S(1)}) custom-call(bf16[32,2048]{1,0:T(8,128)(2,1)S(1)} %copy-done.7, f32[1,2048]{1,0:T(1,128)S(1)} %bitcast.10, bf16[2048,256]{1,0:T(8,128)(2,1)S(1)} %copy-done.2, bf16[2048,256]{1,0:T(8,128)(2,1)S(1)} %copy-done.3, ...), custom_call_target="tpu_custom_call" | custom-call | tf_op jit(solution)/shard_map/proj_state/pallas_call | solution.py:500
  23.3 0.0 copy-done.16
  23.3 0.9 %copy.27.dg_hbm = bf16[2048,352]{1,0:T(8,128)(2,1)S(1)} copy(bf16[2048,352]{0,1:T(8,128)(2,1)S(1)} %copy-done.16) | data formatting | bytes 2883584 | tf_op args[19]
  24.2 0.0 copy-start.8
  24.2 0.0 copy-start.9
  24.2 1.9 %copy.28.du_hbm = bf16[2048,352]{1,0:T(8,128)(2,1)S(1)} copy(bf16[2048,352]{0,1:T(8,128)(2,1)} %param.43) | data formatting | bytes 2883584 | tf_op args[20]
  26.0 0.0 copy-done.8
  26.1 0.0 copy-done.9
  26.1 0.0 copy-start.1
  26.1 1.4 %copy-done.1 = bf16[352,2048]{1,0:T(8,128)(2,1)S(1)} copy-done((bf16[352,2048]{1,0:T(8,128)(2,1)S(1)}, bf16[352,2048]{1,0:T(8,128)(2,1)}, u32[]{:S(2)}) %copy-start.1) | copy-done | bytes 1441816
  27.4 39.2 %exchange.1 = bf16[8,2048]{1,0:T(8,128)(2,1)S(1)} custom-call(bf16[4,8,2048]{2,1,0:T(8,128)(2,1)S(1)} %get-tuple-element.6.part_ref, f32[8,2048]{1,0:T(8,128)S(1)} %get-tuple-element.7.base_ref, f32[8,128]{1,0:T(8,128)S(1)} %get-tuple-element.8.wext_ref, f32[1,2048]{1,0:T(1,128)S(1)} %bitcast.8, f32[1,2048]{1,0:T(1,128)S(1)} %bitcast.9, ...), custom_call_target="tpu_custom_call" | custom-call | tf_op jit(solution)/shard_map/exchange/pallas_call | solution.py:526
  66.6 0.6 copy.30
  (9 shorter events, 0.0 us)
Async XLA Ops:
  2.2 1.6 %copy-start = (f32[32,4,4096]{2,1,0:T(4,128)S(1)}, f32[32,4,4096]{2,1,0:T(4,128)}, u32[]{:S(2)}) copy-start(f32[32,4,4096]{2,1,0:T(4,128)} %state_ref.1) | copy-start | bytes 6291460
  3.8 1.2 %copy-start.2 = (bf16[2048,256]{1,0:T(8,128)(2,1)S(1)}, bf16[2048,256]{1,0:T(8,128)(2,1)}, u32[]{:S(2)}) copy-start(bf16[2048,256]{1,0:T(8,128)(2,1)} %wr_ref.1) | copy-start | bytes 3145732
  5.0 1.2 %copy-start.3 = (bf16[2048,256]{1,0:T(8,128)(2,1)S(1)}, bf16[2048,256]{1,0:T(8,128)(2,1)}, u32[]{:S(2)}) copy-start(bf16[2048,256]{1,0:T(8,128)(2,1)} %wk_ref.1) | copy-start | bytes 3145732
  6.3 1.2 %copy-start.4 = (bf16[2048,256]{1,0:T(8,128)(2,1)S(1)}, bf16[2048,256]{1,0:T(8,128)(2,1)}, u32[]{:S(2)}) copy-start(bf16[2048,256]{1,0:T(8,128)(2,1)} %wv_ref.1) | copy-start | bytes 3145732
  7.5 1.2 %copy-start.5 = (bf16[2048,256]{1,0:T(8,128)(2,1)S(1)}, bf16[2048,256]{1,0:T(8,128)(2,1)}, u32[]{:S(2)}) copy-start(bf16[2048,256]{1,0:T(8,128)(2,1)} %wd_ref.1) | copy-start | bytes 3145732
  8.7 1.2 %copy-start.6 = (bf16[256,2048]{1,0:T(8,128)(2,1)S(1)}, bf16[256,2048]{1,0:T(8,128)(2,1)}, u32[]{:S(2)}) copy-start(bf16[256,2048]{1,0:T(8,128)(2,1)} %wo_ref.1) | copy-start | bytes 3145732
  9.9 0.9 %copy-start.7 = (bf16[32,2048]{1,0:T(8,128)(2,1)S(1)}, bf16[32,2048]{1,0:T(8,128)(2,1)}, u32[]{:S(2)}) copy-start(bf16[32,2048]{1,0:T(8,128)(2,1)} %tokens_ref.1) | copy-start | bytes 393220
  10.8 0.7 %copy-start.10 = (f32[2048]{0:T(1024)S(1)}, f32[2048]{0:T(1024)}, u32[]{:S(2)}) copy-start(f32[2048]{0:T(1024)} %param.25) | copy-start | bytes 24580
  11.5 0.7 %copy-start.11 = (f32[256]{0:T(256)S(1)}, f32[256]{0:T(256)}, u32[]{:S(2)}) copy-start(f32[256]{0:T(256)} %param.30) | copy-start | bytes 3076
  12.2 0.7 %copy-start.12 = (f32[256]{0:T(256)S(1)}, f32[256]{0:T(256)}, u32[]{:S(2)}) copy-start(f32[256]{0:T(256)} %param.31) | copy-start | bytes 3076
  12.9 0.7 %copy-start.13 = (f32[256]{0:T(256)S(1)}, f32[256]{0:T(256)}, u32[]{:S(2)}) copy-start(f32[256]{0:T(256)} %param.32) | copy-start | bytes 3076
  13.6 0.7 %copy-start.14 = (f32[256]{0:T(256)S(1)}, f32[256]{0:T(256)}, u32[]{:S(2)}) copy-start(f32[256]{0:T(256)} %param.33) | copy-start | bytes 3076
  14.2 0.7 %copy-start.15 = (f32[256]{0:T(256)S(1)}, f32[256]{0:T(256)}, u32[]{:S(2)}) copy-start(f32[256]{0:T(256)} %param.34) | copy-start | bytes 3076
  14.9 8.4 %copy-start.16 = (bf16[2048,352]{0,1:T(8,128)(2,1)S(1)}, bf16[2048,352]{0,1:T(8,128)(2,1)}, u32[]{:S(2)}) copy-start(bf16[2048,352]{0,1:T(8,128)(2,1)} %param.42) | copy-start | bytes 4325380
  24.2 1.9 %copy-start.8 = (f32[2048]{0:T(1024)S(1)}, f32[2048]{0:T(1024)}, u32[]{:S(2)}) copy-start(f32[2048]{0:T(1024)} %param.36) | copy-start | bytes 24580
  24.2 1.9 %copy-start.9 = (f32[2048]{0:T(1024)S(1)}, f32[2048]{0:T(1024)}, u32[]{:S(2)}) copy-start(f32[2048]{0:T(1024)} %param.45) | copy-start | bytes 24580
  26.1 1.4 %copy-start.1 = (bf16[352,2048]{1,0:T(8,128)(2,1)S(1)}, bf16[352,2048]{1,0:T(8,128)(2,1)}, u32[]{:S(2)}) copy-start(bf16[352,2048]{1,0:T(8,128)(2,1)} %dd_hbm.1) | copy-start | bytes 4325380

commit v2 on v1

--- a/solution.py
+++ b/solution.py
@@ -8,6 +8,7 @@
 from jax.sharding import PartitionSpec as P
 
 HEAD_WIDTH = 64
+VMEM_BYTES = 67043328
 
 
 PRECISE = lax.Precision.HIGHEST
@@ -204,12 +205,18 @@
     return (layer_out, next_state)
 
 
-def proj_state_kernel(
-    tokens_ref, gain_ref, wr_ref, wk_ref, wv_ref, wd_ref, doff_ref, coff_ref, cfac_ref,
-    own_ref, hgain_ref, wo_ref, routes_ref, rweight_ref, state_ref,
-    next_ref, part_ref, base_ref, wext_ref,
-    sbuf, nbuf, in_sem, out_sem,
-):
+def proj_state_kernel(count, *refs):
+    sources, refs = refs[:count], refs[count:]
+    state_ref, next_ref, part_ref, base_ref, wext_ref = refs[:5]
+    held, (sbuf, nbuf, arg_sem, in_sem, out_sem) = refs[5 : 5 + count], refs[5 + count :]
+    (tokens_ref, gain_ref, wr_ref, wk_ref, wv_ref, wd_ref, doff_ref, coff_ref, cfac_ref,
+     own_ref, hgain_ref, routes_ref, rweight_ref, wo_ref) = held
+    pulls = [
+        pltpu.make_async_copy(src, dst, arg_sem.at[i])
+        for i, (src, dst) in enumerate(zip(sources, held))
+    ]
+    for pull in pulls:
+        pull.start()
     seqs, width = tokens_ref.shape
     heads = state_ref.shape[1]
     lanes = part_ref.shape[0]
@@ -220,14 +227,22 @@
     for load in loads:
         load.start()
     f32, bf16 = jnp.float32, jnp.bfloat16
+    for pull in pulls[:2]:
+        pull.wait()
     toks = tokens_ref[...].astype(f32)
     normed = (
         toks * lax.rsqrt(jnp.mean(toks * toks, axis=-1, keepdims=True) + 1e-06) * gain_ref[...]
     ).astype(bf16)
+    pulls[2].wait()
     recept = jnp.dot(normed, wr_ref[...], preferred_element_type=f32)
+    pulls[3].wait()
     keys = jnp.dot(normed, wk_ref[...], preferred_element_type=f32)
+    pulls[4].wait()
     values = jnp.dot(normed, wv_ref[...], preferred_element_type=f32)
+    pulls[5].wait()
     logits = jnp.dot(normed, wd_ref[...], preferred_element_type=f32)
+    for pull in pulls[6:]:
+        pull.wait()
     decay = jnp.exp(-jnp.exp(doff_ref[...] + logits))
     rate = jax.nn.sigmoid(coff_ref[...] + cfac_ref[...] * keys)
     key_in = keys * rate
@@ -303,14 +318,22 @@
         part_ref[i] = mine.astype(bf16)
         base = jnp.where(me_lane == i, mine + toks[i * rows : (i + 1) * rows], base)
     base_ref[...] = base
-    start = pl.multiple_of(lax.axis_index("ep") * seqs + me_lane * rows, 8)
-    own_start = pl.multiple_of(me_lane * rows, 8)
-    routes = routes_ref[pl.ds(start, rows), :]
-    weights = rweight_ref[pl.ds(own_start, rows), :]
+    start = lax.axis_index("ep") * seqs + me_lane * rows
+
+    def picked_column(ref, k, first):
+        spot = lax.broadcasted_iota(jnp.int32, (rows, ref.shape[1]), 1)
+        wanted = spot == first + lax.broadcasted_iota(jnp.int32, spot.shape, 0)
+        entries = ref[k : k + 1, :].astype(f32)
+        return jnp.sum(jnp.where(wanted, entries, 0.0), axis=-1, keepdims=True)
+
     column = lax.broadcasted_iota(jnp.int32, (rows, 128), 1) % 64
+    column = column.astype(f32)
     table = jnp.zeros((rows, 128), f32)
-    for k in range(routes.shape[1]):
-        table = table + jnp.where(column == routes[:, k : k + 1], weights[:, k : k + 1], 0.0)
+    for k in range(routes_ref.shape[0]):
+        expert = picked_column(routes_ref, k, start)
+        table = table + jnp.where(
+            column == expert, picked_column(rweight_ref, k, me_lane * rows), 0.0
+        )
     wext_ref[...] = table
     for store in stores:
         store.wait()
@@ -318,10 +341,10 @@
 
 def exchange_kernel(
     groups, lanes,
-    part_ref, base_ref, wext_ref, gain_ref, goff_ref,
+    part_ref, base_ref, wext_ref, gain_hbm, goff_hbm,
     eg_hbm, eu_hbm, ed_hbm, dg_hbm, du_hbm, dd_hbm,
     out_ref,
-    eg, eu, ed, dg, du, dd, p_in, xs, flat, hid, dens, ys, y_in, z_in, v_out, v_in,
+    eg, eu, ed, dg, du, dd, gain, goff, hid_rows, p_in, xs, flat, hid, dens, ys, y_in, z_in, v_out, v_in,
     w_sem, s1, r1, sz, rz, st, rt, sc, rc, sa, ra, sb, rb, sv, rv,
 ):
     f32, bf16 = jnp.float32, jnp.bfloat16
@@ -348,7 +371,7 @@
     pulls = [
         pltpu.make_async_copy(src, dst, w_sem.at[i])
         for i, (src, dst) in enumerate(
-            [(dg_hbm, dg), (du_hbm, du), (dd_hbm, dd), (eg_hbm.at[0], eg), (eu_hbm.at[0], eu),
+            [(gain_hbm, gain), (goff_hbm, goff), (dg_hbm, dg), (du_hbm, du), (dd_hbm, dd), (eg_hbm.at[0], eg), (eu_hbm.at[0], eu),
              (ed_hbm.at[0], ed)]
         )
     ]
@@ -371,8 +394,11 @@
         copy.wait_recv()
         hidden = hidden + p_in[d].astype(f32)
     sent += firsts
+    hid_rows[...] = hidden
+    for pull in pulls[:2]:
+        pull.wait()
     normed = hidden * lax.rsqrt(jnp.mean(hidden * hidden, axis=-1, keepdims=True) + 1e-06)
-    xs[0, 0, 0, :, :width] = (normed * gain_ref[...]).astype(bf16)
+    xs[0, 0, 0, :, :width] = (normed * gain[...]).astype(bf16)
     table = wext_ref[...]
     high = table.astype(bf16).astype(f32)
     first_half = lax.broadcasted_iota(jnp.int32, table.shape, 1) < 64
@@ -405,12 +431,13 @@
     mine = gathered(0)
     flat[0:block] = mine.astype(bf16)
     own_rows = mine[:, :width].astype(bf16)
-    for pull in pulls[:3]:
+    for pull in pulls[2:5]:
         pull.wait()
-    gate = jnp.dot(own_rows, dg[...], preferred_element_type=f32)
-    up = jnp.dot(own_rows, du[...], preferred_element_type=f32)
+    across = (((1,), (1,)), ((), ()))
+    gate = lax.dot_general(own_rows, dg[...], across, preferred_element_type=f32)
+    up = lax.dot_general(own_rows, du[...], across, preferred_element_type=f32)
     mixed = (jax.nn.silu(gate) * up).astype(bf16)
-    dens[...] = jnp.dot(mixed, dd[...], preferred_element_type=f32) * jax.nn.sigmoid(goff_ref[...])
+    dens[...] = jnp.dot(mixed, dd[...], preferred_element_type=f32) * jax.nn.sigmoid(goff[...])
     for q in range(zs):
         for d in range(1, lanes):
             hold_t[d, q].wait_recv()
@@ -419,7 +446,7 @@
         for q in range(zs):
             hold_c[d, q].wait_recv()
         flat[d * block : (d + 1) * block] = gathered(d).astype(bf16)
-    for pull in pulls[3:]:
+    for pull in pulls[5:]:
         pull.wait()
     tile = 256
 
@@ -434,46 +461,58 @@
     tail = flat[:, width:].astype(f32)
     picked = lax.broadcasted_iota(jnp.int32, tail.shape, 1) % 64 == me_g
     scale = jnp.sum(jnp.where(picked, tail, 0.0), axis=-1, keepdims=True)
-    wide = 256
-
-    @pl.loop(0, width // wide)
-    def _(n):
-        cols = pl.ds(pl.multiple_of(n * wide, wide), wide)
+    pieces, wide = ys.shape[0], ys.shape[-1]
+    to_core, to_lane, to_z = [], [], []
+
+    def pass_on(n):
+        to_core[n].wait_recv()
+        own = []
+        for d in range(1, lanes):
+            ys[n, 0, d] = (ys[n, 0, d].astype(f32) + y_in[n, d].astype(f32)).astype(bf16)
+            i = n * (lanes - 1) + d - 1
+            own.append(
+                send(ys.at[n, 0, d], z_in.at[n, d - 1], sb.at[i], rb.at[i], lane_peer(-d))
+            )
+        to_lane.append(own)
+
+    for n in range(pieces):
+        cols = slice(n * wide, (n + 1) * wide)
         made = jnp.dot(hid[...], ed[:, cols], preferred_element_type=f32) * scale
         for d in range(lanes):
             piece = made[d * block : (d + 1) * block]
             if d == 0:
                 piece = piece + dens[:, cols]
-            ys[:, d, :, :, cols] = piece.reshape(2, zs, rows, wide).astype(bf16)
-
-    to_core = [
-        send(ys.at[1, d], y_in.at[d], sa.at[d], ra.at[d], partner)
-        for d in list(range(1, lanes)) + [0]
-    ]
-    to_lane = []
-    for d in range(1, lanes):
-        to_core[d - 1].wait_recv()
-        ys[0, d] = (ys[0, d].astype(f32) + y_in[d].astype(f32)).astype(bf16)
-        to_lane.append(
-            send(ys.at[0, d], z_in.at[d - 1], sb.at[d - 1], rb.at[d - 1], lane_peer(-d))
-        )
-    to_core[lanes - 1].wait_recv()
-    total = ys[0, 0].astype(f32) + y_in[0].astype(f32)
-    for d in range(1, lanes):
-        to_lane[d - 1].wait_recv()
-        total = total + z_in[d - 1].astype(f32)
-    v_out[...] = total.astype(bf16)
-    to_z = [
-        send(v_out.at[d], v_in.at[d - 1], sv.at[d - 1], rv.at[d - 1], z_peer(-d))
-        for d in range(1, zs)
-    ]
-    result = hidden + total[0]
-    for d, copy in enumerate(to_z):
-        copy.wait_recv()
-        result = result + v_in[d].astype(f32)
-    out_ref[...] = result.astype(bf16)
+            ys[n, :, d] = piece.reshape(2, zs, rows, wide).astype(bf16)
+        to_core.append(send(ys.at[n, 1], y_in.at[n], sa.at[n], ra.at[n], partner))
+        if n > 0:
+            pass_on(n - 1)
+    pass_on(pieces - 1)
+    for n in range(pieces):
+        cols = slice(n * wide, (n + 1) * wide)
+        total = ys[n, 0, 0].astype(f32) + y_in[n, 0].astype(f32)
+        for d in range(1, lanes):
+            to_lane[n][d - 1].wait_recv()
+            total = total + z_in[n, d - 1].astype(f32)
+        v_out[n] = total.astype(bf16)
+        own = []
+        for d in range(1, zs):
+            i = n * (zs - 1) + d - 1
+            own.append(
+                send(v_out.at[n, d], v_in.at[n, d - 1], sv.at[i], rv.at[i], z_peer(-d))
+            )
+        to_z.append(own)
+        hid_rows[:, cols] = hid_rows[:, cols] + total[0]
+    for n in range(pieces):
+        cols = slice(n * wide, (n + 1) * wide)
+        result = hid_rows[:, cols]
+        for d, copy in enumerate(to_z[n]):
+            copy.wait_recv()
+            result = result + v_in[n, d].astype(f32)
+        out_ref[:, cols] = result.astype(bf16)
     sent += list(hold_z.values()) + list(hold_t.values()) + list(hold_c.values())
-    sent += to_core + to_lane + to_z
+    sent += to_core
+    for own in to_lane + to_z:
+        sent += own
     for copy in sent:
         copy.wait_send()
 
@@ -490,77 +529,87 @@
     heads, flat_width = recurrent_head_state.shape[1:]
     groups, lanes = lax.axis_size("ep"), lax.axis_size("tp")
     rows, zs = seqs // lanes, groups // 2
+    handed = lanes * rows * width * 2 + rows * width * 4 + rows * 128 * 4
+    grant = VMEM_BYTES - handed
     vmem = pl.BlockSpec(memory_space=pltpu.VMEM)
-    anywhere = pl.BlockSpec(memory_space=pl.ANY)
+    anywhere = pl.BlockSpec(memory_space=pltpu.HBM)
     dma = pltpu.SemaphoreType.DMA
 
     def row(vector):
         return vector.reshape(1, -1)
 
+    operands = (
+        tokens, row(first_norm_gain), receptance_matrix, key_matrix, value_matrix, decay_matrix,
+        row(decay_offset), row(correction_offset), row(correction_key_factor),
+        row(own_term_weight), row(head_norm_gain), routing.T, routing_weight.T, output_matrix,
+    )
+    count = len(operands)
     next_state, part, base, table = pl.pallas_call(
-        proj_state_kernel,
+        functools.partial(proj_state_kernel, count),
         out_shape=(
             jax.ShapeDtypeStruct(recurrent_head_state.shape, f32),
             jax.ShapeDtypeStruct((lanes, rows, width), bf16),
             jax.ShapeDtypeStruct((rows, width), f32),
             jax.ShapeDtypeStruct((rows, 128), f32),
         ),
-        in_specs=[vmem] * 14 + [anywhere],
+        in_specs=[anywhere] * (count + 1),
         out_specs=(anywhere, vmem, vmem, vmem),
-        scratch_shapes=[
+        scratch_shapes=[pltpu.VMEM(operand.shape, operand.dtype) for operand in operands]
+        + [
             pltpu.VMEM((heads, seqs, flat_width), f32),
             pltpu.VMEM((heads, seqs, flat_width), f32),
+            dma((count,)),
             dma((heads,)),
             dma((heads,)),
         ],
-        compiler_params=pltpu.CompilerParams(vmem_limit_bytes=40 * 1024 * 1024),
+        compiler_params=pltpu.CompilerParams(vmem_limit_bytes=grant),
         name="proj_state",
-    )(
-        tokens, row(first_norm_gain), receptance_matrix, key_matrix, value_matrix, decay_matrix,
-        row(decay_offset), row(correction_offset), row(correction_key_factor),
-        row(own_term_weight), row(head_norm_gain), output_matrix, routing, routing_weight,
-        recurrent_head_state,
-    )
+    )(*operands, recurrent_head_state)
     hidden_units = expert_gate_weight.shape[2]
+    pieces = 4
+    wide = width // pieces
     total = groups * seqs
     layer_out = pl.pallas_call(
         functools.partial(exchange_kernel, groups, lanes),
         out_shape=jax.ShapeDtypeStruct((rows, width), bf16),
-        in_specs=[vmem] * 5 + [anywhere] * 6,
+        in_specs=[vmem] * 3 + [anywhere] * 8,
         out_specs=vmem,
         scratch_shapes=[
             pltpu.VMEM(expert_gate_weight.shape[1:], bf16),
             pltpu.VMEM(expert_up_weight.shape[1:], bf16),
             pltpu.VMEM(expert_down_weight.shape[1:], bf16),
-            pltpu.VMEM(dense_gate_weight.shape, bf16),
-            pltpu.VMEM(dense_up_weight.shape, bf16),
+            pltpu.VMEM(dense_gate_weight.shape[::-1], bf16),
+            pltpu.VMEM(dense_up_weight.shape[::-1], bf16),
             pltpu.VMEM(dense_down_weight.shape, bf16),
+            pltpu.VMEM((1, width), f32),
+            pltpu.VMEM((1, width), f32),
+            pltpu.VMEM((rows, width), f32),
             pltpu.VMEM((lanes - 1, rows, width), bf16),
             pltpu.VMEM((2, lanes, zs, rows, width + 128), bf16),
             pltpu.VMEM((total, width + 128), bf16),
             pltpu.VMEM((total, hidden_units), bf16),
             pltpu.VMEM((2 * zs * rows, width), f32),
-            pltpu.VMEM((2, lanes, zs, rows, width), bf16),
-            pltpu.VMEM((lanes, zs, rows, width), bf16),
-            pltpu.VMEM((lanes - 1, zs, rows, width), bf16),
-            pltpu.VMEM((zs, rows, width), bf16),
-            pltpu.VMEM((zs - 1, rows, width), bf16),
-            dma((6,)),
+            pltpu.VMEM((pieces, 2, lanes, zs, rows, wide), bf16),
+            pltpu.VMEM((pieces, lanes, zs, rows, wide), bf16),
+            pltpu.VMEM((pieces, lanes - 1, zs, rows, wide), bf16),
+            pltpu.VMEM((pieces, zs, rows, wide), bf16),
+            pltpu.VMEM((pieces, zs - 1, rows, wide), bf16),
+            dma((8,)),
             dma((lanes - 1,)), dma((lanes - 1,)),
             dma((zs - 1,)), dma((zs - 1,)),
             dma(((lanes - 1) * zs,)), dma(((lanes - 1) * zs,)),
             dma((lanes * zs,)), dma((lanes * zs,)),
-            dma((lanes,)), dma((lanes,)),
-            dma((lanes - 1,)), dma((lanes - 1,)),
-            dma((zs - 1,)), dma((zs - 1,)),
+            dma((pieces,)), dma((pieces,)),
+            dma((pieces * (lanes - 1),)), dma((pieces * (lanes - 1),)),
+            dma((pieces * (zs - 1),)), dma((pieces * (zs - 1),)),
         ],
         compiler_params=pltpu.CompilerParams(
-            collective_id=0, has_side_effects=True, vmem_limit_bytes=48 * 1024 * 1024
+            collective_id=0, has_side_effects=True, vmem_limit_bytes=grant - rows * width * 2
         ),
         name="exchange",
     )(
         part, base, table, row(second_norm_gain), row(dense_gate_offset), expert_gate_weight,
-        expert_up_weight, expert_down_weight, dense_gate_weight, dense_up_weight,
+        expert_up_weight, expert_down_weight, dense_gate_weight.T, dense_up_weight.T,
         dense_down_weight,
     )
     return (layer_out, next_state)

time: 67.8 us -> 49.8 us (0.73)
  local copies, waits for them, and re-layouts: 19 us -> 1.38 us
    unnamed x39 -> x1, local copies, waits for them, and re-layouts: 19 us -> 1.38 us
    pallas_call x1, Pallas kernels: 8.35 us -> 9.77 us  [fused(): pl.pallas_call(functools.partial(proj_state_kernel, count), out_shape=(ja...]
    pallas_call x1, Pallas kernels: 39.2 us -> 37.8 us  [fused(): pl.pallas_call(functools.partial(exchange_kernel, groups, lanes), out_sha...]
where the time goes in v2:
time: 49.8 us; the launch traced here: 49.6 us
  Pallas kernels  47.6 us (96%)
  local copies, waits for them, and re-layouts  1.38 us (3%)
  between operations  0.65 us (1%)
    pallas_call x1, Pallas kernels, fused(): pl.pallas_call(functools.partial(exchange_kernel, groups, lanes), out_sha...  37.8 us
    pallas_call x1, Pallas kernels, fused(): pl.pallas_call(functools.partial(proj_state_kernel, count), out_shape=(ja...  9.77 us
    unnamed x1, local copies, waits for them, and re-layouts  1.38 us

profile of v2, /device:TPU:0, one launch (start us, length us, event | category | flops | bytes accessed | tf_op | source)
XLA Modules:
  0.0 49.6 jit_solution(17277510533980922524)
XLA Ops:
  0.6 9.8 %proj_state.1 = (f32[32,4,4096]{2,1,0:T(4,128)}, bf16[4,8,2048]{2,1,0:T(8,128)(2,1)}, f32[8,2048]{1,0:T(8,128)}, f32[8,128]{1,0:T(8,128)}) custom-call(bf16[32,2048]{1,0:T(8,128)(2,1)} %refs_0_.1, f32[1,2048]{1,0:T(1,128)} %bitcast.14, bf16[2048,256]{1,0:T(8,128)(2,1)} %refs_2_.1, bf16[2048,256]{1,0:T(8,128)(2,1)} %refs_3_.1, bf16[2048,256]{1,0:T(8,128)(2,1)} %refs_4_.1, ...), custom_call_target="tpu_custom_call" | custom-call | tf_op jit(solution)/shard_map/proj_state/pallas_call | solution.py:547
  10.4 37.8 %exchange.1 = bf16[8,2048]{1,0:T(8,128)(2,1)} custom-call(bf16[4,8,2048]{2,1,0:T(8,128)(2,1)} %get-tuple-element.6.part_ref, f32[8,2048]{1,0:T(8,128)} %get-tuple-element.7.base_ref, f32[8,128]{1,0:T(8,128)} %get-tuple-element.8.wext_ref, f32[1,2048]{1,0:T(1,128)} %bitcast.15, f32[1,2048]{1,0:T(1,128)} %bitcast.16, bf16[1,2048,1024]{2,1,0:T(8,128)(2,1)} %eg_hbm.1, ...), custom_call_target="tpu_custom_call" | custom-call | tf_op jit(solution)/shard_map/exchange/pallas_call | solution.py:572
  48.2 1.4 %copy.26 = bf16[8,2048]{1,0:T(8,128)(2,1)} copy(bf16[8,2048]{1,0:T(8,128)(2,1)} %exchange.1) | data formatting | bytes 65536
